TPU v7x, 32 devices: a whole 2x2x4 slice. The times are simulated.
32 devices in a mesh: grp: 2 (over y), sp: 4 (over z), tp: 4 (over x, core).
Axes of the slice: x: 2, y: 2, z: 4, core: 2. Of those that a mesh axis runs over, the one named last changes fastest.
Arguments:
- query_nope: bfloat16 [2560, 1024], P(('grp', 'sp'), 'tp'), parts along dimension 0, may hold values from -12 to 12
- query_rope: bfloat16 [2560, 512], P(('grp', 'sp'), 'tp'), parts along dimension 0, may hold values from -48 to 48
- token_latent: bfloat16 [2560, 256], P(('grp', 'sp')), parts along dimension 0, may hold values from -6 to 6
- key_rope: bfloat16 [2560, 32], P(('grp', 'sp')), parts along dimension 0, may hold values from -48 to 48
- latent_norm_gain: float32 [256], replicated, may hold values from 0.1 to 1.9
- key_expand_weight: bfloat16 [256, 1024], replicated, may hold values from -0.375 to 0.375
- value_expand_weight: bfloat16 [256, 1024], replicated, may hold values from -0.375 to 0.375
- residual: bfloat16 [2560, 2048], P(('grp', 'sp')), parts along dimension 0, may hold values from -3 to 3
- out_weight: bfloat16 [1024, 2048], P('tp'), may hold values from -0.375 to 0.375
- ffn_gain: float32 [2048], replicated, may hold values from 0.1 to 1.9
- gate_weight: bfloat16 [2048, 5632], P('sp', 'tp'), may hold values from -0.125 to 0.125
- up_weight: bfloat16 [2048, 5632], P('sp', 'tp'), may hold values from -0.125 to 0.125
- down_weight: bfloat16 [5632, 2048], P('tp', 'sp'), may hold values from -0.078125 to 0.078125
Outputs:
- layer_output: bfloat16 [2560, 2048], P(('grp', 'sp', 'tp')), parts along dimension 0
There are 2 independent parts, one for each index of `grp`. A program takes and returns all parts, laid end to end along the dimension named above; an argument that names none is the same for every part. Nothing has to cross between parts.
All inputs are finite; a program needn't handle non-finite values.
Results may differ from a plain program's by a relative error of at most 0.015.
Values may be sent and summed in bfloat16 or wider, within the bound.
A program may use at most 128 MiB of HBM per device.

v0:
```python
import jax
import jax.numpy as jnp
from jax import lax
from jax.sharding import PartitionSpec as P

UNROTATED_SIZE = 64
ROPE = 32
VALUE_SIZE = 64
GRID_W = 64


def norm_rows(values, gain):
    wide = values.astype(jnp.float32)
    return wide * lax.rsqrt(jnp.mean(wide * wide, axis=-1, keepdims=True) + 1e-06) * gain


def turn_heads(vectors, positions):
    tokens, heads, width = vectors.shape
    freqs = width // 4
    grid_pos = jnp.stack([positions // GRID_W, positions % GRID_W], axis=-1).astype(jnp.float32)
    inverse = jnp.power(10000.0, -jnp.arange(freqs, dtype=jnp.float32) / freqs)
    angles = grid_pos[:, :, None] * inverse
    cosine = jnp.cos(angles)[:, None]
    sine = jnp.sin(angles)[:, None]
    viewed = vectors.reshape(tokens, heads, 2, 2, freqs)
    first = viewed[..., 0, :]
    second = viewed[..., 1, :]
    turned = jnp.stack([first * cosine - second * sine, first * sine + second * cosine], axis=-2)
    return turned.reshape(tokens, heads, width)


def local(
    query_nope,
    query_rope,
    token_latent,
    key_rope,
    latent_norm_gain,
    key_expand_weight,
    value_expand_weight,
    residual,
    out_weight,
    ffn_gain,
    gate_weight,
    up_weight,
    down_weight,
):
    tok_rows = query_nope.shape[0]
    heads_here = query_nope.shape[1] // UNROTATED_SIZE
    own_rows = tok_rows // lax.axis_size("tp")
    tp_index = lax.axis_index("tp")
    positions = lax.axis_index("sp") * tok_rows + jnp.arange(tok_rows, dtype=jnp.int32)
    query_flat = query_nope.reshape(tok_rows, heads_here, UNROTATED_SIZE)
    query_turned = turn_heads(
        query_rope.astype(jnp.float32).reshape(tok_rows, heads_here, ROPE), positions
    ).astype(jnp.bfloat16)
    latent = norm_rows(token_latent, latent_norm_gain).astype(jnp.bfloat16)
    key_turned = turn_heads(key_rope.astype(jnp.float32)[:, None, :], positions)[:, 0].astype(
        jnp.bfloat16
    )
    key_cols = lax.dynamic_slice_in_dim(
        key_expand_weight, tp_index * heads_here * UNROTATED_SIZE, heads_here * UNROTATED_SIZE, 1
    )
    value_cols = lax.dynamic_slice_in_dim(
        value_expand_weight, tp_index * heads_here * VALUE_SIZE, heads_here * VALUE_SIZE, 1
    )
    score_scale = (UNROTATED_SIZE + ROPE) ** (-0.5)

    def absorb(carried, block_in):
        latent_block, rope_block = block_in
        block_rows = latent_block.shape[0]
        key_rows = jnp.dot(latent_block, key_cols, preferred_element_type=jnp.float32).astype(
            jnp.bfloat16
        )
        key_rows = key_rows.reshape(block_rows, heads_here, UNROTATED_SIZE)
        value_rows = jnp.dot(latent_block, value_cols, preferred_element_type=jnp.float32).astype(
            jnp.bfloat16
        )
        value_rows = value_rows.reshape(block_rows, heads_here, VALUE_SIZE)
        scores = (
            jnp.einsum("qhd,khd->hqk", query_flat, key_rows, preferred_element_type=jnp.float32)
            + jnp.einsum(
                "qhd,kd->hqk", query_turned, rope_block, preferred_element_type=jnp.float32
            )
        ) * score_scale
        highest, totals, accumulated = carried
        new_highest = jnp.maximum(highest, jnp.max(scores, axis=-1))
        shrink = jnp.exp(highest - new_highest)
        weights = jnp.exp(scores - new_highest[:, :, None])
        totals = totals * shrink + jnp.sum(weights, axis=-1)
        accumulated = accumulated * shrink.T[:, :, None] + jnp.einsum(
            "hqk,khd->qhd",
            weights.astype(jnp.bfloat16),
            value_rows,
            preferred_element_type=jnp.float32,
        )
        return ((new_highest, totals, accumulated), None)

    initial = (
        jnp.full((heads_here, tok_rows), -jnp.inf, jnp.float32),
        jnp.zeros((heads_here, tok_rows), jnp.float32),
        jnp.zeros((tok_rows, heads_here, VALUE_SIZE), jnp.float32),
    )
    carried = initial
    latent_piece = lax.all_gather(latent, "sp", axis=0, tiled=True)
    rope_piece = lax.all_gather(key_turned, "sp", axis=0, tiled=True)
    shard_count = latent_piece.shape[0] // tok_rows
    grouped = max(
        (
            factor
            for factor in range(1, shard_count + 1)
            if shard_count % factor == 0 and factor * tok_rows <= max(1024, tok_rows)
        )
    )
    block_rows = grouped * tok_rows
    blocks = (
        latent_piece.reshape(-1, block_rows, latent_piece.shape[1]),
        rope_piece.reshape(-1, block_rows, rope_piece.shape[1]),
    )
    carried, _ = lax.scan(absorb, carried, blocks)
    highest, totals, accumulated = carried
    attended = (
        (accumulated / totals.T[:, :, None])
        .reshape(tok_rows, heads_here * VALUE_SIZE)
        .astype(jnp.bfloat16)
    )
    projected = jnp.dot(attended, out_weight, preferred_element_type=jnp.float32).astype(
        jnp.bfloat16
    )
    summed = lax.psum(projected, "tp").astype(jnp.float32)
    mixed_all = residual.astype(jnp.float32) + summed
    normed_all = norm_rows(mixed_all, ffn_gain).astype(jnp.bfloat16)
    mixed_own = lax.dynamic_slice_in_dim(mixed_all, tp_index * own_rows, own_rows, 0)
    gate_piece = lax.all_gather(gate_weight, "sp", axis=0, tiled=True)
    up_piece = lax.all_gather(up_weight, "sp", axis=0, tiled=True)
    gate = jnp.dot(normed_all, gate_piece, preferred_element_type=jnp.float32)
    up_part = jnp.dot(normed_all, up_piece, preferred_element_type=jnp.float32)
    hidden = (jax.nn.silu(gate) * up_part).astype(jnp.bfloat16)
    terms = jnp.dot(
        hidden,
        lax.all_gather(down_weight, "sp", axis=1, tiled=True),
        preferred_element_type=jnp.float32,
    )
    ffn_own = lax.psum_scatter(
        terms.astype(jnp.bfloat16), "tp", scatter_dimension=0, tiled=True
    ).astype(jnp.float32)
    return (mixed_own + ffn_own).astype(jnp.bfloat16)


def solution(mesh):
    return jax.shard_map(
        local,
        mesh=mesh,
        in_specs=(
            P(("grp", "sp"), "tp"),
            P(("grp", "sp"), "tp"),
            P(("grp", "sp"), None),
            P(("grp", "sp"), None),
            P(),
            P(),
            P(),
            P(("grp", "sp"), None),
            P("tp", None),
            P(),
            P("sp", "tp"),
            P("sp", "tp"),
            P("tp", "sp"),
        ),
        out_specs=P(("grp", "sp", "tp"), None),
        check_vma=False,
    )
```

profile of v0, /device:TPU:0, one launch (start us, length us, event | category | flops | bytes accessed | tf_op | source)
XLA Modules:
  0.0 428.1 jit_solution(11533256106749414533)
XLA Ops:
  7.4 1.1 copy.26
  8.6 0.7 convert.18
  9.7 15.1 %all-gather = bf16[4,320,32]{1,2,0:T(8,128)(2,1)S(1)} all-gather(bf16[1,320,32]{1,2,0:T(8,128)(2,1)S(1)} %bitcast.82), channel_id=1, replica_groups=mesh['grp'=2,'sp'=4,'tp'=4] {'sp'}, dimensions={0}, use_global_device_ids=true | all-gather | bytes 102400 | tf_op jit(solution)/shard_map/all_gather | solution.py:105
  25.0 1.1 fusion.24
  26.1 1.0 fusion.26
  27.1 16.8 %all_gather.15 = bf16[1280,256]{1,0:T(8,128)(2,1)S(1)} all-gather(bf16[320,256]{1,0:T(8,128)(2,1)S(1)} %fusion.26), channel_id=1, replica_groups=mesh['grp'=2,'sp'=4,'tp'=4] {'sp'}, dimensions={0}, use_global_device_ids=true | all-gather | bytes 819200 | tf_op jit(solution)/shard_map/all_gather | solution.py:104
  44.2 1.0 constant_dynamic-slice_fusion
  45.2 15.2 %while.15 = (s32[]{:T(128)}, f32[4,320]{1,0:T(4,128)S(1)}, f32[4,320]{1,0:T(4,128)S(1)}, f32[320,4,64]{0,2,1:T(8,128)S(1)}, bf16[2,640,256]{2,1,0:T(8,128)(2,1)S...) while((s32[]{:T(128)}, f32[4,320]{1,0:T(4,128)S(1)}, ...), condition=%wide.region_4.5_spmd.clone, body=%wide.region_1.4_spmd.clone.sunk | while | flops 436231680 | bytes 32759976 | solution.py:119
  46.1 2.4 fusion.75
  48.8 2.9 fusion.79
  51.8 1.0 fusion.77
  53.7 2.4 fusion.75
  56.4 2.9 fusion.79
  59.3 1.0 fusion.77
  60.4 1.6 convolution_convert_fusion.3
  63.9 37.3 %all-reduce.2.cloned.1.call-done = bf16[320,2048]{1,0:T(8,128)(2,1)} async-done(((bf16[320,2048]{1,0:T(8,128)(2,1)}), bf16[320,2048]{1,0:T(8,128)(2,1)}) %all-reduce.2.cloned.1.call-update) | async-done | bytes 1310736 | tf_op jit(solution)/shard_map/psum | solution.py:129
  101.1 3.2 convert_add_fusion
  104.4 66.1 %all-gather.5.cloned.1.call-done = bf16[2048,1408]{1,0:T(8,128)(2,1)} async-done(((bf16[512,1408]{1,0:T(8,128)(2,1)}), bf16[2048,1408]{1,0:T(8,128)(2,1)}) %all-gather.5.cloned.1.call-update) | async-done | bytes 5767184 | tf_op jit(solution)/shard_map/all_gather | solution.py:133
  170.5 6.5 %fusion.36 = f32[320,1408]{1,0:T(8,128)} fusion(bf16[2048,1408]{1,0:T(8,128)(2,1)} %all-gather.5.cloned.1.call-done, f32[2048]{0:T(1024)S(1)} %copy-done.4, f32[320]{0:T(512)S(1)} %add_rsqrt_fusion, bf16[320,2048]{1,0:T(8,128)(2,1)} %all-reduce.2.cloned.1.call-done, bf16[320,2048]{1,0:T(8,128)(2,1)S(1)} %copy-done.2), kind=kOutput, calls=%fused_computation.69 | convolution fusion | flops 1849425920 | bytes 10200320 | tf_op jit(solution)/shard_map/dot_general | solution.py:135
  177.0 99.7 %all-gather.7.cloned.1.call-done = bf16[2048,1408]{1,0:T(8,128)(2,1)} async-done(((bf16[512,1408]{1,0:T(8,128)(2,1)}), bf16[2048,1408]{1,0:T(8,128)(2,1)}) %all-gather.7.cloned.1.call-update) | async-done | bytes 5767184 | tf_op jit(solution)/shard_map/all_gather | solution.py:134
  276.8 106.3 %all-gather.9.cloned.1.call-done = bf16[1408,2048]{1,0:T(8,128)(2,1)} async-done(((bf16[1408,512]{1,0:T(8,128)(2,1)}), bf16[1408,2048]{1,0:T(8,128)(2,1)}) %all-gather.9.cloned.1.call-update) | async-done | bytes 5767184 | tf_op jit(solution)/shard_map/all_gather | solution.py:140
  383.0 10.7 %convolution_convert_fusion.2 = bf16[320,2048]{1,0:T(8,128)(2,1)} fusion(bf16[1408,2048]{1,0:T(8,128)(2,1)} %all-gather.9.cloned.1.call-done, bf16[2048,1408]{1,0:T(8,128)(2,1)} %all-gather.7.cloned.1.call-done, f32[320,1408]{1,0:T(8,128)} %fusion.36, f32[2048]{0:T(1024)S(1)} %copy-done.4, f32[320]{0:T(512)S(1)} %add_rsqrt_fusion, ...), kind=kOutput, calls=%fused_computation.27 | convolution fusion | flops 3698278400 | bytes 17278208 | tf_op jit(solution)/shard_map/dot_general | solution.py:138
  393.7 24.8 %reduce-scatter.2.cloned.1.call-done = bf16[80,2048]{1,0:T(8,128)(2,1)} async-done(((bf16[320,2048]{1,0:T(8,128)(2,1)}), bf16[80,2048]{1,0:T(8,128)(2,1)}) %reduce-scatter.2.cloned.1.call-update) | async-done | bytes 327696 | tf_op jit(solution)/shard_map/reduce_scatter | solution.py:143
  418.6 2.0 add_convert_fusion
  (53 shorter events, 5.3 us)
Async XLA Ops:
  7.4 53.0 %copy-start = (bf16[256,2048]{1,0:T(8,128)(2,1)S(1)}, bf16[256,2048]{1,0:T(8,128)(2,1)}, u32[]{:S(2)}) copy-start(bf16[256,2048]{1,0:T(8,128)(2,1)} %param.23) | copy-start | bytes 3145732
  7.4 36.6 %copy-start.3 = (bf16[320,256]{1,0:T(8,128)(2,1)S(1)}, bf16[320,256]{1,0:T(8,128)(2,1)}, u32[]{:S(2)}) copy-start(bf16[320,256]{1,0:T(8,128)(2,1)} %param.15) | copy-start | bytes 491524
  7.4 93.8 %all-reduce.2.cloned.1.call-start = ((), (), s32[]{:S(2)}) async-start(), calls=%async_computation.1 | async-start | bytes 2621440 | tf_op jit(solution)/shard_map/psum | solution.py:129
  48.5 3.2 copy-start.1
  56.1 3.2 copy-start.1
  62.0 39.1 %copy-start.2 = (bf16[320,2048]{1,0:T(8,128)(2,1)S(1)}, bf16[320,2048]{1,0:T(8,128)(2,1)}, u32[]{:S(2)}) copy-start(bf16[320,2048]{1,0:T(8,128)(2,1)} %param.22) | copy-start | bytes 3932164
  62.1 108.4 %all-gather.5.cloned.1.call-start = ((), (), s32[]{:S(2)}) async-start(), calls=%async_computation.2 | async-start | bytes 7208960 | tf_op jit(solution)/shard_map/all_gather | solution.py:133
  62.6 214.1 %all-gather.7.cloned.1.call-start = ((), (), s32[]{:S(2)}) async-start(), calls=%async_computation.3 | async-start | bytes 7208960 | tf_op jit(solution)/shard_map/all_gather | solution.py:134
  63.2 319.8 %all-gather.9.cloned.1.call-start = ((), (), s32[]{:S(2)}) async-start(), calls=%async_computation.4 | async-start | bytes 7208960 | tf_op jit(solution)/shard_map/all_gather | solution.py:140
  63.8 106.7 %copy-start.4 = (f32[2048]{0:T(1024)S(1)}, f32[2048]{0:T(1024)}, u32[]{:S(2)}) copy-start(f32[2048]{0:T(1024)} %param.24) | copy-start | bytes 24580
  63.8 354.8 %reduce-scatter.2.cloned.1.call-start = ((), (), s32[]{:S(2)}) async-start(), calls=%async_computation.5 | async-start | bytes 1638400 | tf_op jit(solution)/shard_map/reduce_scatter | solution.py:143
Sparse Core Ops, SparseCore 0:
  62.2 38.9 all-reduce.1
  393.8 24.6 reduce-scatter.1
Sparse Core Ops, SparseCore 1:
  64.1 106.3 all-gather.4
  171.9 104.8 all-gather.6
  278.2 104.8 all-gather.8
where the time goes:
time: 428 us
  waiting for transfers between devices  336 us (79%)
  blocking collectives  31.9 us (7%)
  matrix products  31.9 us (7%)
  between operations  15.2 us (4%)
  other arithmetic  10.5 us (2%)
    all_gather x1, waiting for transfers between devices, local(): lax.all_gather(down_weight, 'sp', axis=1, tiled=True)  106 us
    all_gather x1, waiting for transfers between devices, local(): up_piece = lax.all_gather(up_weight, 'sp', axis=0, tiled=True)  99.7 us
    all_gather x1, waiting for transfers between devices, local(): gate_piece = lax.all_gather(gate_weight, 'sp', axis=0, tiled=True)  66.1 us
    psum x1, waiting for transfers between devices, local(): summed = lax.psum(projected, 'tp').astype(jnp.float32)  37.3 us
    reduce_scatter x1, waiting for transfers between devices, local(): lax.psum_scatter(terms.astype(jnp.bfloat16), 'tp', scatter_dimension=0, t...  24.8 us
    all_gather x1, blocking collectives, local(): latent_piece = lax.all_gather(latent, 'sp', axis=0, tiled=True)  16.8 us
    all_gather x1, blocking collectives, local(): rope_piece = lax.all_gather(key_turned, 'sp', axis=0, tiled=True)  15.1 us
    dot_general x1, matrix products, local(): jnp.dot(hidden, lax.all_gather(down_weight, 'sp', axis=1, tiled=True), pr...  10.7 us
  transfers between devices with their start and end apart: 5, of which 5 were waited for; matrix products, arithmetic and copies ran while one was open for 2% of the time, Pallas kernels for 0%

commit v1 on v0

--- a/solution.py
+++ b/solution.py
@@ -1,3 +1,4 @@
+import functools
 import jax
 import jax.numpy as jnp
 from jax import lax
@@ -7,6 +8,30 @@
 ROPE = 32
 VALUE_SIZE = 64
 GRID_W = 64
+
+
+def lead_frames(z_in, row_axis, where_dim):
+    n_shards = lax.axis_size(row_axis)
+    cards = []
+    for s in range(n_shards):
+        cards.append((s, (s + 1) % n_shards))
+
+    def push_the_sector(clean):
+        if len(clean) == n_shards:
+            return clean
+        big = lax.ppermute(clean[0], axis_name=row_axis, perm=cards)
+        f_next = push_the_sector([big, *clean])
+        return f_next
+
+    base_arr = push_the_sector([z_in])
+    fresh = jnp.concatenate(base_arr, axis=where_dim)
+    block_now = jnp.roll(
+        fresh, shift=(lax.axis_index(row_axis) + 1) * z_in.shape[where_dim], axis=where_dim
+    )
+    return block_now
+
+
+treat_the_scenes = functools.partial(lead_frames, row_axis="sp", where_dim=0)
 
 
 def norm_rows(values, gain):
@@ -130,7 +155,7 @@
     mixed_all = residual.astype(jnp.float32) + summed
     normed_all = norm_rows(mixed_all, ffn_gain).astype(jnp.bfloat16)
     mixed_own = lax.dynamic_slice_in_dim(mixed_all, tp_index * own_rows, own_rows, 0)
-    gate_piece = lax.all_gather(gate_weight, "sp", axis=0, tiled=True)
+    gate_piece = treat_the_scenes(gate_weight)
     up_piece = lax.all_gather(up_weight, "sp", axis=0, tiled=True)
     gate = jnp.dot(normed_all, gate_piece, preferred_element_type=jnp.float32)
     up_part = jnp.dot(normed_all, up_piece, preferred_element_type=jnp.float32)

time: 428 us -> 387 us (0.904)
  waiting for transfers between devices: 336 us -> 259 us
  starting transfers between devices: 0.17 us -> 18.3 us
  local copies, waits for them, and re-layouts: 2.49 us -> 19.2 us
    ppermute x0 -> x3, waiting for transfers between devices: none -> 177 us  [push_the_sector(): big = lax.ppermute(clean[0], axis_name=row_axis, perm=cards)]
    all_gather x1, waiting for transfers between devices: 99.7 us -> 0.01 us  [local(): up_piece = lax.all_gather(up_weight, 'sp', axis=0, tiled=True)]
    all_gather x1 -> x0, waiting for transfers between devices: 66.1 us -> none  [local(): gate_piece = lax.all_gather(gate_weight, 'sp', axis=0, tiled=True)]
    all_gather x1, waiting for transfers between devices: 106 us -> 56.2 us  [local(): lax.all_gather(down_weight, 'sp', axis=1, tiled=True)]
    psum x1, waiting for transfers between devices: 37.3 us -> 0.01 us  [local(): summed = lax.psum(projected, 'tp').astype(jnp.float32)]
    ppermute x0 -> x3, starting transfers between devices: none -> 18.1 us  [push_the_sector(): big = lax.ppermute(clean[0], axis_name=row_axis, perm=cards)]
    unnamed x11 -> x24, local copies, waits for them, and re-layouts: 1.29 us -> 16.8 us
  transfers between devices with their start and end apart: 5 -> 7, of which waited for: 5 -> 5; matrix products, arithmetic and copies ran while one was open for 2% -> 7% of each run, Pallas kernels for 0% -> 0%
where the time goes in v1:
time: 387 us
  waiting for transfers between devices  259 us (67%)
  matrix products  32.3 us (8%)
  blocking collectives  31.9 us (8%)
  local copies, waits for them, and re-layouts  19.2 us (5%)
  starting transfers between devices  18.3 us (5%)
  between operations  15 us (4%)
  other arithmetic  11 us (3%)
    ppermute x3, waiting for transfers between devices, push_the_sector(): big = lax.ppermute(clean[0], axis_name=row_axis, perm=cards)  177 us
    all_gather x1, waiting for transfers between devices, local(): lax.all_gather(down_weight, 'sp', axis=1, tiled=True)  56.2 us
    reduce_scatter x1, waiting for transfers between devices, local(): lax.psum_scatter(terms.astype(jnp.bfloat16), 'tp', scatter_dimension=0, t...  25.4 us
    ppermute x3, starting transfers between devices, push_the_sector(): big = lax.ppermute(clean[0], axis_name=row_axis, perm=cards)  18.1 us
    all_gather x1, blocking collectives, local(): latent_piece = lax.all_gather(latent, 'sp', axis=0, tiled=True)  16.8 us
    unnamed x24, local copies, waits for them, and re-layouts  16.8 us
    all_gather x1, blocking collectives, local(): rope_piece = lax.all_gather(key_turned, 'sp', axis=0, tiled=True)  15.1 us
    dot_general x1, matrix products, local(): jnp.dot(hidden, lax.all_gather(down_weight, 'sp', axis=1, tiled=True), pr...  10.6 us
  transfers between devices with their start and end apart: 7, of which 5 were waited for; matrix products, arithmetic and copies ran while one was open for 7% of the time, Pallas kernels for 0%

profile of v1, /device:TPU:0, one launch (start us, length us, event | category | flops | bytes accessed | tf_op | source)
XLA Modules:
  0.0 387.0 jit_solution(9562380086568254285)
XLA Ops:
  9.7 15.1 %all-gather = bf16[4,320,32]{1,2,0:T(8,128)(2,1)S(1)} all-gather(bf16[1,320,32]{1,2,0:T(8,128)(2,1)S(1)} %bitcast.81), channel_id=1, replica_groups=mesh['grp'=2,'sp'=4,'tp'=4] {'sp'}, dimensions={0}, use_global_device_ids=true | all-gather | bytes 102400 | tf_op jit(solution)/shard_map/all_gather | solution.py:130
  27.1 16.8 %all_gather.12 = bf16[1280,256]{1,0:T(8,128)(2,1)S(1)} all-gather(bf16[320,256]{1,0:T(8,128)(2,1)S(1)} %fusion.32), channel_id=1, replica_groups=mesh['grp'=2,'sp'=4,'tp'=4] {'sp'}, dimensions={0}, use_global_device_ids=true | all-gather | bytes 819200 | tf_op jit(solution)/shard_map/all_gather | solution.py:129
  45.2 15.2 %while.15 = (s32[]{:T(128)}, f32[4,320]{1,0:T(4,128)S(1)}, f32[4,320]{1,0:T(4,128)S(1)}, f32[320,4,64]{0,2,1:T(8,128)S(1)}, bf16[2,640,256]{2,1,0:T(8,128)(2,1)S...) while((s32[]{:T(128)}, f32[4,320]{1,0:T(4,128)S(1)}, ...), condition=%wide.region_4.5_spmd.clone, body=%wide.region_1.4_spmd.clone.sunk | while | flops 436231680 | bytes 32759976 | solution.py:144
  46.1 2.4 fusion.82
  48.8 2.9 fusion.86
  53.7 2.4 fusion.82
  56.4 2.9 fusion.86
  60.4 1.6 convolution_convert_fusion.3
  63.5 52.6 %collective-permute-done = bf16[512,1408]{1,0:T(8,128)(2,1)S(1)} collective-permute-done((bf16[512,1408]{1,0:T(8,128)(2,1)S(1)}, bf16[512,1408]{1,0:T(8,128)(2,1)S(1)}, u32[]{:S(2)}, u32[]{:S(2)}) %collective-permute-start) | collective-permute-done | bytes 1441824 | tf_op jit(solution)/shard_map/ppermute | solution.py:22
  117.3 13.5 %collective-permute-start.1 = (bf16[512,1408]{1,0:T(8,128)(2,1)S(1)}, bf16[512,1408]{1,0:T(8,128)(2,1)}, u32[]{:S(2)}, u32[]{:S(2)}) collective-permute-start(bf16[512,1408]{1,0:T(8,128)(2,1)S(1)} %collective-permute-done), channel_id=1, source_target_pairs={{0,4},{4,8},{8,12},{12,0},{1,5},{5,9},{9,13},{13,1},{2,6},{6,10},{... | collective-permute-start | bytes 4325384 | tf_op jit(solution)/shard_map/ppermute | solution.py:22
  130.8 75.2 %collective-permute-done.1 = bf16[512,1408]{1,0:T(8,128)(2,1)} collective-permute-done((bf16[512,1408]{1,0:T(8,128)(2,1)S(1)}, bf16[512,1408]{1,0:T(8,128)(2,1)}, u32[]{:S(2)}, u32[]{:S(2)}) %collective-permute-start.1) | collective-permute-done | bytes 1441824 | tf_op jit(solution)/shard_map/ppermute | solution.py:22
  206.0 4.5 %collective-permute-start.2 = (bf16[512,1408]{1,0:T(8,128)(2,1)}, bf16[512,1408]{1,0:T(8,128)(2,1)}, u32[]{:S(2)}, u32[]{:S(2)}) collective-permute-start(bf16[512,1408]{1,0:T(8,128)(2,1)} %collective-permute-done.1), channel_id=1, source_target_pairs={{0,4},{4,8},{8,12},{12,0},{1,5},{5,9},{9,13},{13,1},{2,6},{6,10},{... | collective-permute-start | bytes 4325384 | tf_op jit(solution)/shard_map/ppermute | solution.py:22
  210.5 3.7 convert_add_fusion
  214.2 48.7 %collective-permute-done.2 = bf16[512,1408]{1,0:T(8,128)(2,1)} collective-permute-done((bf16[512,1408]{1,0:T(8,128)(2,1)}, bf16[512,1408]{1,0:T(8,128)(2,1)}, u32[]{:S(2)}, u32[]{:S(2)}) %collective-permute-start.2) | collective-permute-done | bytes 1441824 | tf_op jit(solution)/shard_map/ppermute | solution.py:22
  262.9 2.6 constant_dynamic-update-slice_fusion.7
  265.5 2.6 constant_dynamic-update-slice_fusion.6
  270.6 2.6 constant_dynamic-update-slice_fusion.3
  273.2 2.7 constant_dynamic-update-slice_fusion.2
  275.8 1.3 constant_dynamic-update-slice_fusion.1
  278.3 7.0 %fusion.44 = f32[320,1408]{1,0:T(8,128)} fusion(bf16[2048,1408]{1,0:T(8,128)(2,1)} %all-gather.4.cloned.1.call-done, f32[2048]{0:T(1024)S(1)} %copy-done.7, f32[320]{0:T(512)S(1)} %add_rsqrt_fusion, bf16[320,2048]{1,0:T(8,128)(2,1)} %all-reduce.2.cloned.1.call-done, bf16[320,2048]{1,0:T(8,128)(2,1)} %param.22), kind=kOutput, calls=%fused_computation.80 | convolution fusion | flops 1849425920 | bytes 10200320 | tf_op jit(solution)/shard_map/dot_general | solution.py:161
  285.4 56.2 %all-gather.6.cloned.1.call-done = bf16[1408,2048]{1,0:T(8,128)(2,1)} async-done(((bf16[1408,512]{1,0:T(8,128)(2,1)}), bf16[1408,2048]{1,0:T(8,128)(2,1)}) %all-gather.6.cloned.1.call-update) | async-done | bytes 5767184 | tf_op jit(solution)/shard_map/all_gather | solution.py:165
  341.6 10.6 %convolution_convert_fusion.2 = bf16[320,2048]{1,0:T(8,128)(2,1)} fusion(bf16[1408,2048]{1,0:T(8,128)(2,1)} %all-gather.6.cloned.1.call-done, f32[320,1408]{1,0:T(8,128)} %fusion.44, bf16[4096,1408]{1,0:T(8,128)(2,1)} %constant_dynamic-update-slice_fusion, s32[]{:T(128)S(6)} %select_n.57, f32[2048]{0:T(1024)S(1)} %copy-done.7, f32[320]{0:T(512)S(1)} %add_rsqrt_fusion, ...), kind=kOutput, calls=%fused_computation.28 | convolution fusion | flops 3698278400 | bytes 17278212 | tf_op jit(solution)/shard_map/dot_general | solution.py:163
  352.2 25.4 %reduce-scatter.2.cloned.1.call-done = bf16[80,2048]{1,0:T(8,128)(2,1)} async-done(((bf16[320,2048]{1,0:T(8,128)(2,1)}), bf16[80,2048]{1,0:T(8,128)(2,1)}) %reduce-scatter.2.cloned.1.call-update) | async-done | bytes 327696 | tf_op jit(solution)/shard_map/reduce_scatter | solution.py:168
  377.6 2.0 add_convert_fusion
  (70 shorter events, 16.7 us)
Async XLA Ops:
  7.4 53.0 %copy-start = (bf16[256,2048]{1,0:T(8,128)(2,1)S(1)}, bf16[256,2048]{1,0:T(8,128)(2,1)}, u32[]{:S(2)}) copy-start(bf16[256,2048]{1,0:T(8,128)(2,1)} %param.23) | copy-start | bytes 3145732
  7.4 36.6 %copy-start.6 = (bf16[320,256]{1,0:T(8,128)(2,1)S(1)}, bf16[320,256]{1,0:T(8,128)(2,1)}, u32[]{:S(2)}) copy-start(bf16[320,256]{1,0:T(8,128)(2,1)} %param.15) | copy-start | bytes 491524
  7.4 203.1 %all-reduce.2.cloned.1.call-start = ((), (), s32[]{:S(2)}) async-start(), calls=%async_computation.1 | async-start | bytes 2621440 | tf_op jit(solution)/shard_map/psum | solution.py:154
  48.5 3.2 copy-start.1
  56.1 3.2 copy-start.1
  62.0 1.4 copy-start.2
  62.0 216.3 %all-gather.4.cloned.1.call-start = ((), (), s32[]{:S(2)}) async-start(), calls=%async_computation.2 | async-start | bytes 7208960 | tf_op jit(solution)/shard_map/all_gather | solution.py:159
  62.6 278.9 %all-gather.6.cloned.1.call-start = ((), (), s32[]{:S(2)}) async-start(), calls=%async_computation.3 | async-start | bytes 7208960 | tf_op jit(solution)/shard_map/all_gather | solution.py:165
  63.2 314.4 %reduce-scatter.2.cloned.1.call-start = ((), (), s32[]{:S(2)}) async-start(), calls=%async_computation.4 | async-start | bytes 1638400 | tf_op jit(solution)/shard_map/reduce_scatter | solution.py:168
  63.4 52.7 %collective-permute-start = (bf16[512,1408]{1,0:T(8,128)(2,1)S(1)}, bf16[512,1408]{1,0:T(8,128)(2,1)S(1)}, u32[]{:S(2)}, u32[]{:S(2)}) collective-permute-start(bf16[512,1408]{1,0:T(8,128)(2,1)S(1)} %copy-done.2), channel_id=1, source_target_pairs={{0,4},{4,8},{8,12},{12,0},{1,5},{5,9},{9,13},{13,1},{2,6},{6,10},{... | collective-permute-start | bytes 4325384 | tf_op jit(solution)/shard_map/ppermute | solution.py:22
  116.1 1.2 copy-start.3
  117.3 88.7 %collective-permute-start.1 = (bf16[512,1408]{1,0:T(8,128)(2,1)S(1)}, bf16[512,1408]{1,0:T(8,128)(2,1)}, u32[]{:S(2)}, u32[]{:S(2)}) collective-permute-start(bf16[512,1408]{1,0:T(8,128)(2,1)S(1)} %collective-permute-done), channel_id=1, source_target_pairs={{0,4},{4,8},{8,12},{12,0},{1,5},{5,9},{9,13},{13,1},{2,6},{6,10},{... | collective-permute-start | bytes 4325384 | tf_op jit(solution)/shard_map/ppermute | solution.py:22
  206.0 56.9 %collective-permute-start.2 = (bf16[512,1408]{1,0:T(8,128)(2,1)}, bf16[512,1408]{1,0:T(8,128)(2,1)}, u32[]{:S(2)}, u32[]{:S(2)}) collective-permute-start(bf16[512,1408]{1,0:T(8,128)(2,1)} %collective-permute-done.1), channel_id=1, source_target_pairs={{0,4},{4,8},{8,12},{12,0},{1,5},{5,9},{9,13},{13,1},{2,6},{6,10},{... | collective-permute-start | bytes 4325384 | tf_op jit(solution)/shard_map/ppermute | solution.py:22
  214.2 53.9 %copy-start.4 = (bf16[512,1408]{1,0:T(8,128)(2,1)S(1)}, bf16[512,1408]{1,0:T(8,128)(2,1)}, u32[]{:S(2)}) copy-start(bf16[512,1408]{1,0:T(8,128)(2,1)} %copy-done.3) | copy-start | bytes 4325380
  275.8 2.5 copy-start.7
  278.3 63.3 %copy-start.5 = (bf16[320,2048]{1,0:T(8,128)(2,1)S(1)}, bf16[320,2048]{1,0:T(8,128)(2,1)}, u32[]{:S(2)}) copy-start(bf16[320,2048]{1,0:T(8,128)(2,1)} %param.22) | copy-start | bytes 3932164
Sparse Core Ops, SparseCore 0:
  62.2 38.8 all-reduce.1
  352.3 25.2 reduce-scatter.1
Sparse Core Ops, SparseCore 1:
  64.1 160.0 all-gather.3
  225.6 115.9 all-gather.5
